TPU v7x, 32 devices: a whole 2x2x4 slice. The times are simulated.
32 devices in a mesh: rep: 4 (over z), fs: 2 (over y), tp: 4 (over x, core).
Axes of the slice: x: 2, y: 2, z: 4, core: 2. Of those that a mesh axis runs over, the one named last changes fastest.
Arguments:
- inputs: bfloat16 [512, 4096], P('rep'), may hold values from -6 to 6
- cotangent: bfloat16 [512, 4096], P('rep'), may hold values from -6 to 6
- w_gate: bfloat16 [4096, 11264], P(None, ('fs', 'tp')), may hold values from -0.09375 to 0.09375
- w_upward: bfloat16 [4096, 11264], P(None, ('fs', 'tp')), may hold values from -0.09375 to 0.09375
- w_down: bfloat16 [11264, 4096], P(('fs', 'tp')), may hold values from -0.0546875 to 0.0546875
Outputs:
- grad_input: bfloat16 [512, 4096], P('rep')
- grad_gate: float32 [4096, 11264], P('rep', ('fs', 'tp'))
- grad_upward: float32 [4096, 11264], P('rep', ('fs', 'tp'))
- grad_down: float32 [11264, 4096], P(('fs', 'tp'), 'rep')
All inputs are finite; a program needn't handle non-finite values.
Results may differ from a plain program's by a relative error of at most 0.0049.
Values may be sent and summed in bfloat16 or wider, within the bound.
A program may use at most 128 MiB of HBM per device.

v0:
```python
import jax
import jax.numpy as jnp
from jax import lax
from jax.sharding import PartitionSpec as P


def contract_rows(left, right):
    return lax.dot_general(
        left, right, (((0,), (0,)), ((), ())), preferred_element_type=jnp.float32
    )


def contract_cols(left, right):
    return lax.dot_general(
        left, right, (((1,), (1,)), ((), ())), preferred_element_type=jnp.float32
    )


def local(inputs, cotangent, w_gate, w_upward, w_down):
    gate_pre = jnp.dot(inputs, w_gate, preferred_element_type=jnp.float32)
    up_pre = jnp.dot(inputs, w_upward, preferred_element_type=jnp.float32)
    sigmoid_gate = jax.nn.sigmoid(gate_pre)
    activated = gate_pre * sigmoid_gate
    hidden = (activated * up_pre).astype(jnp.bfloat16)
    hidden_grad = contract_cols(cotangent, w_down)
    gate_delta = (
        hidden_grad * up_pre * sigmoid_gate * (1.0 + gate_pre * (1.0 - sigmoid_gate))
    ).astype(jnp.bfloat16)
    up_delta = (hidden_grad * activated).astype(jnp.bfloat16)
    input_cols, cotangent_cols = (
        lax.all_to_all(inputs, "rep", split_axis=1, concat_axis=0, tiled=True),
        lax.all_to_all(cotangent, "rep", split_axis=1, concat_axis=0, tiled=True),
    )
    piece_gate = lax.all_gather(gate_delta, "rep", axis=0, tiled=True)
    piece_up = lax.all_gather(up_delta, "rep", axis=0, tiled=True)
    piece_hidden = lax.all_gather(hidden, "rep", axis=0, tiled=True)
    grad_gate = contract_rows(input_cols, piece_gate)
    grad_upward = contract_rows(input_cols, piece_up)
    grad_down = contract_rows(piece_hidden, cotangent_cols)
    input_terms = contract_cols(gate_delta, w_gate) + contract_cols(up_delta, w_upward)
    grad_input = lax.psum(input_terms, ("fs", "tp")).astype(jnp.bfloat16)
    return (grad_input, grad_gate, grad_upward, grad_down)


def solution(mesh):
    in_specs = (
        P("rep", None),
        P("rep", None),
        P(None, ("fs", "tp")),
        P(None, ("fs", "tp")),
        P(("fs", "tp"), None),
    )
    out_specs = (
        P("rep", None),
        P("rep", ("fs", "tp")),
        P("rep", ("fs", "tp")),
        P(("fs", "tp"), "rep"),
    )
    return jax.shard_map(local, mesh=mesh, in_specs=in_specs, out_specs=out_specs, check_vma=False)
```

profile of v0, /device:TPU:0, one launch (start us, length us, event | category | flops | bytes accessed | tf_op | source)
XLA Modules:
  0.0 190.2 jit_solution(5874101361756558968)
XLA Ops:
  7.2 0.0 copy-start.2
  7.2 0.0 all-gather.4.cloned.1.call-start
  7.2 0.0 copy-start
  7.2 8.6 %fusion.1 = f32[128,1408]{1,0:T(8,128)S(1)} fusion(bf16[128,4096]{1,0:T(8,128)(2,1)} %param.6, bf16[1408,4096]{1,0:T(8,128)(2,1)} %param.9), kind=kOutput, calls=%fused_computation.8 | convolution fusion | flops 1476395008 | bytes 13303808 | tf_op jit(solution)/shard_map/dot_general | solution.py:14
  15.8 0.0 copy-done.2
  15.8 0.0 copy-done
  15.8 0.0 copy-start.1
  15.8 1.8 fusion.2
  17.7 2.4 %copy-done.1 = bf16[4096,1408]{1,0:T(8,128)(2,1)S(1)} copy-done((bf16[4096,1408]{1,0:T(8,128)(2,1)S(1)}, bf16[4096,1408]{1,0:T(8,128)(2,1)}, u32[]{:S(2)}) %copy-start.1) | copy-done | bytes 11534360
  20.1 3.0 %multiply_convert_fusion = (bf16[128,1408]{1,0:T(8,128)(2,1)}, bf16[128,1408]{1,0:T(8,128)(2,1)}, bf16[128,1408]{1,0:T(8,128)(2,1)}) fusion(f32[128,1408]{1,0:T(8,128)S(1)} %fusion.2, f32[128,1408]{1,0:T(8,128)S(1)} %fusion.1, bf16[128,4096]{1,0:T(8,128)(2,1)S(1)} %copy-done.2, bf16[4096,1408]{1,0:T(8,128)(2,1)S(1)} %copy-done.1), kind=kOutput, calls=%fused_computation.3 | convolution fusion | flops 1479098368 | bytes 15106048 | tf_op jit(solution)/shard_map/dot_general | solution.py:21
  23.1 0.0 copy-start.3
  23.1 0.0 copy-start.4
  23.1 0.0 all-gather.4.cloned.1.call-update
  23.1 0.0 all-gather.6.cloned.1.call-start
  23.2 0.7 all-gather.6.cloned.1.call-update
  23.9 1.3 copy.13
  25.2 6.3 %all-to-all-start = ((bf16[128,4,1024]{0,2,1:T(8,128)(2,1)}), bf16[128,4,1024]{0,2,1:T(8,128)(2,1)S(1)}, u32[]{:S(2)}, u32[]{:S(2)}) async-start(bf16[128,4,1024]{0,2,1:T(8,128)(2,1)} %bitcast.27), calls=%async_computation | async-start | bytes 2097152 | tf_op jit(solution)/shard_map/all_to_all | solution.py:31
  31.5 0.0 all-gather.8.cloned.1.call-start
  31.5 0.7 all-gather.8.cloned.1.call-update
  32.3 0.0 copy-done.3
  32.3 1.3 copy.15
  33.6 0.0 copy-done.4
  33.6 9.5 %fusion.3 = f32[128,4096]{1,0:T(8,128)} fusion(bf16[128,1408]{1,0:T(8,128)(2,1)S(1)} %copy-done.4, bf16[4096,1408]{1,0:T(8,128)(2,1)} %param.7), kind=kOutput, calls=%fused_computation.10 | convolution fusion | flops 1476395008 | bytes 13991936 | tf_op jit(solution)/shard_map/dot_general | solution.py:14
  43.1 37.0 %all-to-all-done = bf16[128,4,1024]{0,2,1:T(8,128)(2,1)S(1)} async-done(((bf16[128,4,1024]{0,2,1:T(8,128)(2,1)}), bf16[128,4,1024]{0,2,1:T(8,128)(2,1)S(1)}, u32[]{:S(2)}, u32[]{:S(2)}) %all-to-all-start) | async-done | bytes 1048608 | tf_op jit(solution)/shard_map/all_to_all | solution.py:31
  80.1 4.3 %all-to-all-start.1 = ((bf16[128,4,1024]{0,2,1:T(8,128)(2,1)}), bf16[128,4,1024]{0,2,1:T(8,128)(2,1)}, u32[]{:S(2)}, u32[]{:S(2)}) async-start(bf16[128,4,1024]{0,2,1:T(8,128)(2,1)} %bitcast.5), calls=%async_computation.1 | async-start | bytes 2097152 | tf_op jit(solution)/shard_map/all_to_all | solution.py:32
  84.3 9.0 %convolution_add_fusion = f32[128,4096]{1,0:T(8,128)S(1)} fusion(f32[128,4096]{1,0:T(8,128)} %fusion.3, bf16[128,1408]{1,0:T(8,128)(2,1)} %get-tuple-element.18, bf16[4096,1408]{1,0:T(8,128)(2,1)} %param.8), kind=kOutput, calls=%fused_computation | convolution fusion | flops 1476919296 | bytes 16089088 | tf_op jit(solution)/shard_map/dot_general | solution.py:14
  93.3 59.1 %all-reduce.1 = bf16[128,4096]{1,0:T(8,128)(2,1)} all-reduce(f32[128,4096]{1,0:T(8,128)S(1)} %convolution_add_fusion), channel_id=1, replica_groups=mesh['rep'=4,'fs'=2,'tp'=4] {'fs','tp'}, use_global_device_ids=true, to_apply=%region_0.0 | all-reduce | flops 524288 | bytes 3145728 | tf_op jit(solution)/shard_map/psum | solution.py:41
  152.4 0.5 copy.14
  153.0 0.0 all-to-all-done.1
  153.0 1.5 copy.16
  154.5 0.0 all-gather.4.cloned.1.call-done
  154.5 5.6 %convolution_bitcast_fusion.1 = f32[1024,1408]{0,1:T(8,128)} fusion(bf16[512,1408]{1,0:T(8,128)(2,1)} %all-gather.4.cloned.1.call-done, bf16[512,1024]{1,0:T(8,128)(2,1)S(1)} %bitcast.29), kind=kOutput, calls=%fused_computation.2 | convolution fusion | flops 1476395008 | bytes 8257536 | tf_op jit(solution)/shard_map/dot_general | solution.py:8
  160.1 6.2 %copy.17 = f32[1024,1408]{1,0:T(8,128)} copy(f32[1024,1408]{0,1:T(8,128)} %convolution_bitcast_fusion.1) | data formatting | bytes 11534336
  166.3 0.0 all-gather.6.cloned.1.call-done
  166.3 5.6 %convolution_bitcast_fusion = f32[1024,1408]{0,1:T(8,128)} fusion(bf16[512,1408]{1,0:T(8,128)(2,1)} %all-gather.6.cloned.1.call-done, bf16[512,1024]{1,0:T(8,128)(2,1)S(1)} %bitcast.30), kind=kOutput, calls=%fused_computation.1 | convolution fusion | flops 1476395008 | bytes 8257536 | tf_op jit(solution)/shard_map/dot_general | solution.py:8
  171.9 6.2 %copy.18 = f32[1024,1408]{1,0:T(8,128)} copy(f32[1024,1408]{0,1:T(8,128)} %convolution_bitcast_fusion) | data formatting | bytes 11534336
  178.1 0.0 all-gather.8.cloned.1.call-done
  178.1 5.6 %fusion.4 = f32[1408,1024]{1,0:T(8,128)} fusion(bf16[512,1408]{1,0:T(8,128)(2,1)} %all-gather.8.cloned.1.call-done, bf16[512,1024]{1,0:T(8,128)(2,1)S(1)} %bitcast.28), kind=kOutput, calls=%fused_computation.11 | convolution fusion | flops 1476395008 | bytes 8257536 | tf_op jit(solution)/shard_map/dot_general | solution.py:8
Async XLA Ops:
  7.2 8.6 %copy-start.2 = (bf16[128,4096]{1,0:T(8,128)(2,1)S(1)}, bf16[128,4096]{1,0:T(8,128)(2,1)}, u32[]{:S(2)}) copy-start(bf16[128,4096]{1,0:T(8,128)(2,1)} %param.5) | copy-start | bytes 3145732
  7.2 147.3 %all-gather.4.cloned.1.call-start = ((), (), s32[]{:S(2)}) async-start(), calls=%async_computation.2 | async-start | bytes 1802240 | tf_op jit(solution)/shard_map/all_gather | solution.py:34
  7.2 8.6 %copy-start = (bf16[4096,1408]{1,0:T(8,128)(2,1)S(1)}, bf16[4096,1408]{1,0:T(8,128)(2,1)}, u32[]{:S(2)}) copy-start(bf16[4096,1408]{1,0:T(8,128)(2,1)} %param.7) | copy-start | bytes 34603012
  15.8 4.3 %copy-start.1 = (bf16[4096,1408]{1,0:T(8,128)(2,1)S(1)}, bf16[4096,1408]{1,0:T(8,128)(2,1)}, u32[]{:S(2)}) copy-start(bf16[4096,1408]{1,0:T(8,128)(2,1)} %param.8) | copy-start | bytes 34603012
  23.1 9.2 %copy-start.3 = (bf16[128,4096]{1,0:T(8,128)(2,1)S(1)}, bf16[128,4096]{1,0:T(8,128)(2,1)}, u32[]{:S(2)}) copy-start(bf16[128,4096]{1,0:T(8,128)(2,1)} %param.6) | copy-start | bytes 3145732
  23.1 10.5 %copy-start.4 = (bf16[128,1408]{1,0:T(8,128)(2,1)S(1)}, bf16[128,1408]{1,0:T(8,128)(2,1)}, u32[]{:S(2)}) copy-start(bf16[128,1408]{1,0:T(8,128)(2,1)} %get-tuple-element.17) | copy-start | bytes 1081348
  23.1 143.2 %all-gather.6.cloned.1.call-start = ((), (), s32[]{:S(2)}) async-start(), calls=%async_computation.3 | async-start | bytes 1802240 | tf_op jit(solution)/shard_map/all_gather | solution.py:35
  25.2 54.9 %all-to-all-start = ((bf16[128,4,1024]{0,2,1:T(8,128)(2,1)}), bf16[128,4,1024]{0,2,1:T(8,128)(2,1)S(1)}, u32[]{:S(2)}, u32[]{:S(2)}) async-start(bf16[128,4,1024]{0,2,1:T(8,128)(2,1)} %bitcast.27), calls=%async_computation | async-start | bytes 2097152 | tf_op jit(solution)/shard_map/all_to_all | solution.py:31
  31.5 146.6 %all-gather.8.cloned.1.call-start = ((), (), s32[]{:S(2)}) async-start(), calls=%async_computation.4 | async-start | bytes 1802240 | tf_op jit(solution)/shard_map/all_gather | solution.py:36
  80.1 72.9 %all-to-all-start.1 = ((bf16[128,4,1024]{0,2,1:T(8,128)(2,1)}), bf16[128,4,1024]{0,2,1:T(8,128)(2,1)}, u32[]{:S(2)}, u32[]{:S(2)}) async-start(bf16[128,4,1024]{0,2,1:T(8,128)(2,1)} %bitcast.5), calls=%async_computation.1 | async-start | bytes 2097152 | tf_op jit(solution)/shard_map/all_to_all | solution.py:32
Sparse Core Ops, SparseCore 0:
  23.2 57.4 all-gather.3
  82.3 48.3 all-gather.5
  132.3 33.8 all-gather.7
where the time goes:
time: 191 us; the launch traced here: 190 us
  blocking collectives  59.1 us (31%)
  matrix products  48.6 us (25%)
  waiting for transfers between devices  38.5 us (20%)
  local copies, waits for them, and re-layouts  19.5 us (10%)
  between operations  13.9 us (7%)
  starting transfers between devices  10.7 us (6%)
    psum x1, blocking collectives, local(): grad_input = lax.psum(input_terms, ('fs', 'tp')).astype(jnp.bfloat16)  59.1 us
    all_to_all x1, waiting for transfers between devices, local(): lax.all_to_all(inputs, 'rep', split_axis=1, concat_axis=0, tiled=True)  37 us
    dot_general x3, matrix products, contract_cols(): lax.dot_general(left, right, (((1,), (1,)), ((), ())), preferred_element_...  27 us
    unnamed x14, local copies, waits for them, and re-layouts  17.5 us
    dot_general x3, matrix products, contract_rows(): lax.dot_general(left, right, (((0,), (0,)), ((), ())), preferred_element_...  16.7 us
    all_to_all x1, starting transfers between devices, local(): lax.all_to_all(inputs, 'rep', split_axis=1, concat_axis=0, tiled=True)  6.35 us
    all_to_all x1, starting transfers between devices, local(): lax.all_to_all(cotangent, 'rep', split_axis=1, concat_axis=0, tiled=True)  4.27 us
  transfers between devices with their start and end apart: 5, of which 1 were waited for; matrix products, arithmetic and copies ran while one was open for 25% of the time, Pallas kernels for 0%

commit v1 on v0

--- a/solution.py
+++ b/solution.py
@@ -2,6 +2,12 @@
 import jax.numpy as jnp
 from jax import lax
 from jax.sharding import PartitionSpec as P
+from jax.lax import psum
+
+
+def make_sizes_on_mesh(state, mesh_ax, mesh_name):
+    then = psum(psum(state, mesh_ax), mesh_name)
+    return then
 
 
 def contract_rows(left, right):
@@ -38,7 +44,7 @@
     grad_upward = contract_rows(input_cols, piece_up)
     grad_down = contract_rows(piece_hidden, cotangent_cols)
     input_terms = contract_cols(gate_delta, w_gate) + contract_cols(up_delta, w_upward)
-    grad_input = lax.psum(input_terms, ("fs", "tp")).astype(jnp.bfloat16)
+    grad_input = make_sizes_on_mesh(input_terms, "fs", "tp").astype(jnp.bfloat16)
     return (grad_input, grad_gate, grad_upward, grad_down)
 
 

time: 191 us -> 225 us (1.18)
  waiting for transfers between devices: 38.5 us -> 90.6 us
  blocking collectives: 59.1 us -> 41.5 us
    all_to_all x1, waiting for transfers between devices: 0.01 us -> 42.2 us  [local(): lax.all_to_all(cotangent, 'rep', split_axis=1, concat_axis=0, tiled=True)]
    psum x1, blocking collectives: 59.1 us -> 41.5 us  [make_sizes_on_mesh(): then = psum(psum(state, mesh_ax), mesh_name)]
    all_to_all x1, waiting for transfers between devices: 37 us -> 46.7 us  [local(): lax.all_to_all(inputs, 'rep', split_axis=1, concat_axis=0, tiled=True)]
  transfers between devices with their start and end apart: 5 -> 6, of which waited for: 1 -> 2; matrix products, arithmetic and copies ran while one was open for 25% -> 12% of each run, Pallas kernels for 0% -> 0%
where the time goes in v1:
time: 225 us; the launch traced here: 224 us
  waiting for transfers between devices  90.6 us (40%)
  matrix products  47.7 us (21%)
  blocking collectives  41.5 us (18%)
  local copies, waits for them, and re-layouts  18.6 us (8%)
  between operations  15.8 us (7%)
  starting transfers between devices  9.98 us (4%)
    all_to_all x1, waiting for transfers between devices, local(): lax.all_to_all(inputs, 'rep', split_axis=1, concat_axis=0, tiled=True)  46.7 us
    all_to_all x1, waiting for transfers between devices, local(): lax.all_to_all(cotangent, 'rep', split_axis=1, concat_axis=0, tiled=True)  42.2 us
    psum x1, blocking collectives, make_sizes_on_mesh(): then = psum(psum(state, mesh_ax), mesh_name)  41.5 us
    dot_general x3, matrix products, contract_cols(): lax.dot_general(left, right, (((1,), (1,)), ((), ())), preferred_element_...  26.3 us
    unnamed x14, local copies, waits for them, and re-layouts  17.5 us
    dot_general x3, matrix products, contract_rows(): lax.dot_general(left, right, (((0,), (0,)), ((), ())), preferred_element_...  16.7 us
    all_to_all x1, starting transfers between devices, local(): lax.all_to_all(inputs, 'rep', split_axis=1, concat_axis=0, tiled=True)  6.34 us
  transfers between devices with their start and end apart: 6, of which 2 were waited for; matrix products, arithmetic and copies ran while one was open for 12% of the time, Pallas kernels for 0%

profile of v1, /device:TPU:0, one launch (start us, length us, event | category | flops | bytes accessed | tf_op | source)
XLA Modules:
  0.0 224.1 jit_solution(6366149549941727887)
XLA Ops:
  8.0 0.0 copy-start.2
  8.0 0.0 all-reduce.3.cloned.1.call-start
  8.1 0.0 copy-start
  8.1 8.6 %fusion.1 = f32[128,1408]{1,0:T(8,128)S(1)} fusion(bf16[128,4096]{1,0:T(8,128)(2,1)} %param.6, bf16[1408,4096]{1,0:T(8,128)(2,1)} %param.9), kind=kOutput, calls=%fused_computation.8 | convolution fusion | flops 1476395008 | bytes 13303808 | tf_op jit(solution)/shard_map/dot_general | solution.py:20
  16.6 0.0 copy-done.2
  16.6 0.0 copy-done
  16.7 0.0 copy-start.1
  16.7 1.8 fusion.2
  18.5 2.4 %copy-done.1 = bf16[4096,1408]{1,0:T(8,128)(2,1)S(1)} copy-done((bf16[4096,1408]{1,0:T(8,128)(2,1)S(1)}, bf16[4096,1408]{1,0:T(8,128)(2,1)}, u32[]{:S(2)}) %copy-start.1) | copy-done | bytes 11534360
  20.9 2.9 %multiply_convert_fusion = (bf16[128,1408]{1,0:T(8,128)(2,1)}, bf16[128,1408]{1,0:T(8,128)(2,1)S(1)}, bf16[128,1408]{1,0:T(8,128)(2,1)}) fusion(f32[128,1408]{1,0:T(8,128)S(1)} %fusion.2, f32[128,1408]{1,0:T(8,128)S(1)} %fusion.1, bf16[128,4096]{1,0:T(8,128)(2,1)S(1)} %copy-done.2, bf16[4096,1408]{1,0:T(8,128)(2,1)S(1)} %copy-done.1), kind=kOutput, calls=%fused_computation.3 | convolution fusion | flops 1479098368 | bytes 15106048 | tf_op jit(solution)/shard_map/dot_general | solution.py:27
  23.8 0.0 copy-start.4
  23.8 8.2 %fusion.3 = f32[128,4096]{1,0:T(8,128)S(1)} fusion(bf16[128,1408]{1,0:T(8,128)(2,1)S(1)} %get-tuple-element.17, bf16[4096,1408]{1,0:T(8,128)(2,1)} %param.7), kind=kOutput, calls=%fused_computation.10 | convolution fusion | flops 1476395008 | bytes 13991936 | tf_op jit(solution)/shard_map/dot_general | solution.py:20
  32.0 0.0 copy-done.4
  32.0 9.5 %convolution_add_fusion = f32[128,4096]{1,0:T(8,128)} fusion(f32[128,4096]{1,0:T(8,128)S(1)} %fusion.3, bf16[128,1408]{1,0:T(8,128)(2,1)} %get-tuple-element.18, bf16[4096,1408]{1,0:T(8,128)(2,1)} %param.8), kind=kOutput, calls=%fused_computation | convolution fusion | flops 1476919296 | bytes 16089088 | tf_op jit(solution)/shard_map/dot_general | solution.py:20
  41.5 0.0 copy-start.3
  41.5 0.0 all-reduce.3.cloned.1.call-update
  41.6 0.0 all-gather.4.cloned.1.call-start
  41.6 0.5 all-gather.4.cloned.1.call-update
  42.1 1.3 copy.13
  43.5 6.3 %all-to-all-start = ((bf16[128,4,1024]{0,2,1:T(8,128)(2,1)}), bf16[128,4,1024]{0,2,1:T(8,128)(2,1)S(1)}, u32[]{:S(2)}, u32[]{:S(2)}) async-start(bf16[128,4,1024]{0,2,1:T(8,128)(2,1)} %bitcast), calls=%async_computation | async-start | bytes 2097152 | tf_op jit(solution)/shard_map/all_to_all | solution.py:37
  49.8 0.0 all-gather.6.cloned.1.call-start
  49.8 0.6 all-gather.6.cloned.1.call-update
  50.4 0.0 copy-done.3
  50.4 1.3 copy.15
  51.7 46.7 %all-to-all-done = bf16[128,4,1024]{0,2,1:T(8,128)(2,1)S(1)} async-done(((bf16[128,4,1024]{0,2,1:T(8,128)(2,1)}), bf16[128,4,1024]{0,2,1:T(8,128)(2,1)S(1)}, u32[]{:S(2)}, u32[]{:S(2)}) %all-to-all-start) | async-done | bytes 1048608 | tf_op jit(solution)/shard_map/all_to_all | solution.py:37
  98.4 3.5 %all-to-all-start.1 = ((bf16[128,4,1024]{0,2,1:T(8,128)(2,1)}), bf16[128,4,1024]{0,2,1:T(8,128)(2,1)S(1)}, u32[]{:S(2)}, u32[]{:S(2)}) async-start(bf16[128,4,1024]{0,2,1:T(8,128)(2,1)} %bitcast.5), calls=%async_computation.1 | async-start | bytes 2097152 | tf_op jit(solution)/shard_map/all_to_all | solution.py:38
  101.9 0.0 all-gather.8.cloned.1.call-start
  102.0 0.5 all-gather.8.cloned.1.call-update
  102.5 0.5 copy.14
  103.1 42.2 %all-to-all-done.1 = bf16[128,4,1024]{0,2,1:T(8,128)(2,1)S(1)} async-done(((bf16[128,4,1024]{0,2,1:T(8,128)(2,1)}), bf16[128,4,1024]{0,2,1:T(8,128)(2,1)S(1)}, u32[]{:S(2)}, u32[]{:S(2)}) %all-to-all-start.1) | async-done | bytes 1048608 | tf_op jit(solution)/shard_map/all_to_all | solution.py:38
  145.2 0.5 copy.16
  145.8 0.0 all-reduce.3.cloned.1.call-done
  145.8 41.5 %all-reduce.4 = bf16[128,4096]{1,0:T(8,128)(2,1)} all-reduce(f32[128,4096]{1,0:T(8,128)} %all-reduce.3.cloned.1.call-done), channel_id=1, replica_groups=mesh['rep'=4,'fs'=2,'tp'=4] {'tp'}, use_global_device_ids=true, to_apply=%region_1.0 | all-reduce | flops 524288 | bytes 3145728 | tf_op jit(solution)/shard_map/psum | solution.py:9
  187.3 0.0 all-gather.4.cloned.1.call-done
  187.3 5.6 %convolution_bitcast_fusion.1 = f32[1024,1408]{0,1:T(8,128)} fusion(bf16[512,1408]{1,0:T(8,128)(2,1)} %all-gather.4.cloned.1.call-done, bf16[512,1024]{1,0:T(8,128)(2,1)S(1)} %bitcast.29), kind=kOutput, calls=%fused_computation.2 | convolution fusion | flops 1476395008 | bytes 8257536 | tf_op jit(solution)/shard_map/dot_general | solution.py:14
  192.9 6.2 %copy.17 = f32[1024,1408]{1,0:T(8,128)} copy(f32[1024,1408]{0,1:T(8,128)} %convolution_bitcast_fusion.1) | data formatting | bytes 11534336
  199.1 0.0 all-gather.6.cloned.1.call-done
  199.1 5.6 %convolution_bitcast_fusion = f32[1024,1408]{0,1:T(8,128)} fusion(bf16[512,1408]{1,0:T(8,128)(2,1)} %all-gather.6.cloned.1.call-done, bf16[512,1024]{1,0:T(8,128)(2,1)S(1)} %bitcast.30), kind=kOutput, calls=%fused_computation.1 | convolution fusion | flops 1476395008 | bytes 8257536 | tf_op jit(solution)/shard_map/dot_general | solution.py:14
  204.7 6.2 %copy.18 = f32[1024,1408]{1,0:T(8,128)} copy(f32[1024,1408]{0,1:T(8,128)} %convolution_bitcast_fusion) | data formatting | bytes 11534336
  210.9 0.0 all-gather.8.cloned.1.call-done
  210.9 5.6 %fusion.4 = f32[1408,1024]{1,0:T(8,128)} fusion(bf16[512,1408]{1,0:T(8,128)(2,1)} %all-gather.8.cloned.1.call-done, bf16[512,1024]{1,0:T(8,128)(2,1)S(1)} %bitcast.28), kind=kOutput, calls=%fused_computation.11 | convolution fusion | flops 1476395008 | bytes 8257536 | tf_op jit(solution)/shard_map/dot_general | solution.py:14
Async XLA Ops:
  8.0 8.6 %copy-start.2 = (bf16[128,4096]{1,0:T(8,128)(2,1)S(1)}, bf16[128,4096]{1,0:T(8,128)(2,1)}, u32[]{:S(2)}) copy-start(bf16[128,4096]{1,0:T(8,128)(2,1)} %param.5) | copy-start | bytes 3145732
  8.0 137.8 %all-reduce.3.cloned.1.call-start = ((), (), s32[]{:S(2)}) async-start(), calls=%async_computation.2 | async-start | bytes 4194304 | tf_op jit(solution)/shard_map/psum | solution.py:9
  8.1 8.6 %copy-start = (bf16[4096,1408]{1,0:T(8,128)(2,1)S(1)}, bf16[4096,1408]{1,0:T(8,128)(2,1)}, u32[]{:S(2)}) copy-start(bf16[4096,1408]{1,0:T(8,128)(2,1)} %param.7) | copy-start | bytes 34603012
  16.7 4.3 %copy-start.1 = (bf16[4096,1408]{1,0:T(8,128)(2,1)S(1)}, bf16[4096,1408]{1,0:T(8,128)(2,1)}, u32[]{:S(2)}) copy-start(bf16[4096,1408]{1,0:T(8,128)(2,1)} %param.8) | copy-start | bytes 34603012
  23.8 8.2 %copy-start.4 = (bf16[128,1408]{1,0:T(8,128)(2,1)}, bf16[128,1408]{1,0:T(8,128)(2,1)S(1)}, u32[]{:S(2)}) copy-start(bf16[128,1408]{1,0:T(8,128)(2,1)S(1)} %get-tuple-element.17) | copy-start | bytes 1081348
  41.5 8.8 %copy-start.3 = (bf16[128,4096]{1,0:T(8,128)(2,1)S(1)}, bf16[128,4096]{1,0:T(8,128)(2,1)}, u32[]{:S(2)}) copy-start(bf16[128,4096]{1,0:T(8,128)(2,1)} %param.6) | copy-start | bytes 3145732
  41.6 145.7 %all-gather.4.cloned.1.call-start = ((), (), s32[]{:S(2)}) async-start(), calls=%async_computation.3 | async-start | bytes 1802240 | tf_op jit(solution)/shard_map/all_gather | solution.py:40
  43.5 55.0 %all-to-all-start = ((bf16[128,4,1024]{0,2,1:T(8,128)(2,1)}), bf16[128,4,1024]{0,2,1:T(8,128)(2,1)S(1)}, u32[]{:S(2)}, u32[]{:S(2)}) async-start(bf16[128,4,1024]{0,2,1:T(8,128)(2,1)} %bitcast), calls=%async_computation | async-start | bytes 2097152 | tf_op jit(solution)/shard_map/all_to_all | solution.py:37
  49.8 149.3 %all-gather.6.cloned.1.call-start = ((), (), s32[]{:S(2)}) async-start(), calls=%async_computation.4 | async-start | bytes 1802240 | tf_op jit(solution)/shard_map/all_gather | solution.py:41
  98.4 46.8 %all-to-all-start.1 = ((bf16[128,4,1024]{0,2,1:T(8,128)(2,1)}), bf16[128,4,1024]{0,2,1:T(8,128)(2,1)S(1)}, u32[]{:S(2)}, u32[]{:S(2)}) async-start(bf16[128,4,1024]{0,2,1:T(8,128)(2,1)} %bitcast.5), calls=%async_computation.1 | async-start | bytes 2097152 | tf_op jit(solution)/shard_map/all_to_all | solution.py:38
  101.9 109.0 %all-gather.8.cloned.1.call-start = ((), (), s32[]{:S(2)}) async-start(), calls=%async_computation.5 | async-start | bytes 1802240 | tf_op jit(solution)/shard_map/all_gather | solution.py:42
Sparse Core Ops, SparseCore 0:
  41.7 65.6 all-reduce.2
Sparse Core Ops, SparseCore 1:
  44.2 54.8 all-gather.3
  100.5 46.3 all-gather.5
  148.3 33.7 all-gather.7
